TPU v7x, 256 devices: a whole 4x4x8 slice. The times are simulated.
256 devices in a mesh: ep: 64 (over z, x, core), tp: 4 (over y).
Axes of the slice: x: 4, y: 4, z: 8, core: 2. Of those that a mesh axis runs over, the one named last changes fastest.
Arguments:
- query_rows: bfloat16 [12288, 1024], P('ep', 'tp'), may hold values from -8 to 8
- key_rows: bfloat16 [12288, 1024], P('ep', 'tp'), may hold values from -8 to 8
- value_rows: bfloat16 [12288, 1024], P('ep', 'tp'), may hold values from -6 to 6
- lambdas: float32 [8], P('tp'), may hold values from 0.3 to 0.8
- head_gain: float32 [128], replicated, may hold values from 0.1 to 1.9
- w_out: bfloat16 [1024, 2048], replicated, may hold values from -0.1875 to 0.1875
- moe_rows: bfloat16 [32768, 2048], P('ep'), may hold values from -6 to 6
- ffn_gain: float32 [2048], replicated, may hold values from 0.1 to 1.9
- routes: int32 [32768, 2], P('ep'), may hold values from 0 to 63, all different within a row; in each aligned block of 128 rows (0 to 127, 128 to 255, ...) at most 8 rows name the same one
- group_logits: float32 [32768, 4], P('ep'), may hold values from -8 to 8
- pick_logits: float32 [32768, 2], P('ep'), may hold values from -8 to 8
- w_gate: bfloat16 [64, 2048, 1024], P('ep', None, 'tp'), may hold values from -0.125 to 0.125
- w_up: bfloat16 [64, 2048, 1024], P('ep', None, 'tp'), may hold values from -0.125 to 0.125
- w_down: bfloat16 [64, 1024, 2048], P('ep', 'tp'), may hold values from -0.75 to 0.75
Outputs:
- mixer_out: bfloat16 [12288, 2048], P(('ep', 'tp'))
- moe_out: bfloat16 [32768, 2048], P(('ep', 'tp'))
Inputs may be any that keep to these rules, and one draw needn't show every extreme that they name: `routes`: each row names 2 different experts. In each aligned block of 128 rows (the rows of one device) no expert is named by more than 8 rows; some expert is named by exactly 8 rows of a block.
All inputs are finite; a program needn't handle non-finite values.
Results may differ from a plain program's by a relative error of at most 0.015.
Values may be sent and summed in bfloat16 or wider, within the bound.
A program may use at most 128 MiB of HBM per device.

v0:
```python
import jax
import jax.numpy as jnp
from jax import lax
from jax.sharding import PartitionSpec as P

EPS = 1e-06
HEAD_SCALE = 0.8


def cut_along(x, dim, peers):
    before, after = (x.shape[:dim], x.shape[dim + 1 :])
    return jnp.moveaxis(x.reshape(*before, peers, -1, *after), dim, 0)


def sent_and_summed(x, axis, dim):
    peers = lax.axis_size(axis)
    blocks = lax.all_to_all(cut_along(x, dim, peers), axis, 0, 0, tiled=True)
    return jnp.sum(blocks.astype(jnp.float32), axis=0)


def laid_out(blocks, dim):
    blocks = jnp.moveaxis(blocks, 0, dim)
    dims = blocks.shape
    return blocks.reshape(*dims[:dim], dims[dim] * dims[dim + 1], *dims[dim + 2 :])


def copy_for_each(x, axis):
    peers = lax.axis_size(axis)
    return lax.all_to_all(jnp.broadcast_to(x[None], (peers, *x.shape)), axis, 0, 0, tiled=True)


def gather_directly(x, axis, dim):
    return laid_out(copy_for_each(x, axis), dim)


def rms_rows(values, gain):
    squared = jnp.mean(values * values, axis=-1, keepdims=True)
    return values * lax.rsqrt(squared + EPS) * gain


def slot_index(picks, expert_count, capacity):
    flattened = picks.reshape(picks.shape[0], -1)
    onehot = (flattened[..., None] == jnp.arange(expert_count, dtype=jnp.int32)).astype(jnp.int32)
    before = jnp.cumsum(onehot, axis=1) - onehot
    ranking = jnp.sum(before * onehot, axis=-1)
    return flattened * capacity + ranking


def expert_hidden(arrived, gate_weight, up_weight):
    gate_part = jnp.dot(arrived, gate_weight, preferred_element_type=jnp.float32)
    up_part = jnp.dot(arrived, up_weight, preferred_element_type=jnp.float32)
    return (jax.nn.silu(gate_part) * up_part).astype(jnp.bfloat16)


def local(
    query_rows,
    key_rows,
    value_rows,
    lambdas,
    head_gain,
    w_out,
    moe_rows,
    ffn_gain,
    routes,
    group_logits,
    pick_logits,
    w_gate,
    w_up,
    w_down,
):
    token_count = query_rows.shape[0]
    local_heads = lambdas.shape[0]
    head_qk = query_rows.shape[1] // (2 * local_heads)
    head_v = value_rows.shape[1] // local_heads
    score_scale = head_qk ** (-0.5)
    queries = query_rows.reshape(token_count, local_heads, 2, head_qk)

    def absorb(carried, key_value):
        key_block, value_block = key_value
        running_max, running_sum, running_acc = carried
        scores = (
            jnp.einsum("qhmd,khmd->hmqk", queries, key_block, preferred_element_type=jnp.float32)
            * score_scale
        )
        new_max = jnp.maximum(running_max, jnp.max(scores, axis=-1))
        factor = jnp.exp(running_max - new_max)
        weights = jnp.exp(scores - new_max[..., None])
        running_sum = running_sum * factor + jnp.sum(weights, axis=-1)
        update = jnp.einsum(
            "hmqk,khv->hmqv",
            weights.astype(jnp.bfloat16),
            value_block,
            preferred_element_type=jnp.float32,
        )
        return ((new_max, running_sum, running_acc * factor[..., None] + update), None)

    start_state = (
        jnp.full((local_heads, 2, token_count), -1e30, jnp.float32),
        jnp.zeros((local_heads, 2, token_count), jnp.float32),
        jnp.zeros((local_heads, 2, token_count, head_v), jnp.float32),
    )
    carried = start_state
    key_piece = lax.all_gather(key_rows, "ep", axis=0, tiled=True)
    value_piece = lax.all_gather(value_rows, "ep", axis=0, tiled=True)
    length = key_piece.shape[0]
    block_rows = 1024
    blocks = (
        key_piece.reshape(length // block_rows, block_rows, local_heads, 2, head_qk),
        value_piece.reshape(length // block_rows, block_rows, local_heads, head_v),
    )
    carried, unused = lax.scan(absorb, carried, blocks)
    unused_max, final_sum, final_acc = carried
    averaged = final_acc / final_sum[..., None]
    per_head = averaged[:, 0] - lambdas[:, None, None] * averaged[:, 1]
    normed_heads = rms_rows(per_head, head_gain) * HEAD_SCALE
    attended = (
        jnp.transpose(normed_heads, (1, 0, 2))
        .reshape(token_count, local_heads * head_v)
        .astype(jnp.bfloat16)
    )
    own_weight = lax.dynamic_slice_in_dim(
        w_out, lax.axis_index("tp") * attended.shape[1], attended.shape[1], 0
    )
    mixer_out = sent_and_summed(
        jnp.dot(attended, own_weight, preferred_element_type=jnp.float32).astype(jnp.bfloat16),
        "tp",
        0,
    ).astype(jnp.bfloat16)
    quarters = lax.axis_size("tp")
    own_quarter = lax.axis_index("tp")
    expert_count = lax.axis_size("ep")
    model_width = moe_rows.shape[1]
    quarter_rows = moe_rows.shape[0] // quarters
    top_k = routes.shape[1]
    capacity = max(2, 2 * top_k * quarter_rows // expert_count)
    source_rows = jnp.repeat(jnp.arange(quarter_rows, dtype=jnp.int32), top_k)
    own_picks = lax.dynamic_slice_in_dim(routes, own_quarter * quarter_rows, quarter_rows, 0)
    own_tokens = lax.dynamic_slice_in_dim(moe_rows, own_quarter * quarter_rows, quarter_rows, 0)
    normed = rms_rows(own_tokens.astype(jnp.float32), ffn_gain).astype(jnp.bfloat16)
    own_slots = slot_index(own_picks[None], expert_count, capacity)[0]
    outgoing = (
        jnp.zeros((expert_count * capacity, model_width), jnp.bfloat16)
        .at[own_slots]
        .set(normed[source_rows])
    )
    arrived = lax.all_to_all(
        outgoing.reshape(expert_count, capacity, model_width),
        "ep",
        split_axis=0,
        concat_axis=0,
        tiled=True,
    )
    pieces = gather_directly(arrived, "tp", 0)
    flat_rows = pieces.reshape(-1, model_width)
    hidden = expert_hidden(flat_rows, w_gate[0], w_up[0]).reshape(pieces.shape[0], capacity, -1)
    hidden_flat = hidden.reshape(-1, hidden.shape[-1])
    summed = lax.psum_scatter(
        jnp.dot(hidden_flat, w_down[0], preferred_element_type=jnp.float32).astype(jnp.bfloat16),
        "tp",
        scatter_dimension=0,
        tiled=True,
    )
    returned = lax.all_to_all(
        summed.reshape(expert_count, capacity, model_width),
        "ep",
        split_axis=0,
        concat_axis=0,
        tiled=True,
    )
    picked = returned.reshape(-1, model_width)[own_slots].reshape(quarter_rows, top_k, model_width)
    own_groups = lax.dynamic_slice_in_dim(group_logits, own_quarter * quarter_rows, quarter_rows, 0)
    own_pick_logits = lax.dynamic_slice_in_dim(
        pick_logits, own_quarter * quarter_rows, quarter_rows, 0
    )
    group_count = group_logits.shape[1]
    group_prob = jax.nn.softmax(own_groups, axis=-1)
    group_index = own_picks // (expert_count // group_count)
    matches = (group_index[..., None] == jnp.arange(group_count, dtype=jnp.int32)).astype(
        jnp.float32
    )
    group_share = jnp.sum(group_prob[:, None, :] * matches, axis=-1)
    gate_values = group_share * jax.nn.softmax(own_pick_logits, axis=-1)
    moe_out = jnp.sum(gate_values[..., None] * picked.astype(jnp.float32), axis=1).astype(
        jnp.bfloat16
    )
    return (mixer_out, moe_out)


def solution(mesh):
    return jax.shard_map(
        local,
        mesh=mesh,
        in_specs=(
            P("ep", "tp"),
            P("ep", "tp"),
            P("ep", "tp"),
            P("tp"),
            P(),
            P(),
            P("ep", None),
            P(),
            P("ep", None),
            P("ep", None),
            P("ep", None),
            P("ep", None, "tp"),
            P("ep", None, "tp"),
            P("ep", "tp", None),
        ),
        out_specs=(P(("ep", "tp"), None), P(("ep", "tp"), None)),
        check_vma=False,
    )
```

profile of v0, /device:TPU:1, one launch (start us, length us, event | category | flops | bytes accessed | tf_op | source)
XLA Modules:
  0.0 442.0 jit_solution(13916826065649422579)
XLA Ops:
  11.9 1.2 fusion.18
  13.5 2.0 fusion.20
  15.5 6.2 %scatter_custom_fusion = bf16[512,2048]{1,0:T(8,128)(2,1)S(1)} fusion(s32[256]{0:T(256)S(1)} %bitcast.113, bf16[128,2048]{1,0:T(8,128)(2,1)} %fusion.20, s32[1024]{0:T(1024)S(1)} %pad_clamp_fusion.1, bf16[]{:T(256)} %constant.43.clone.1), kind=kCustom, calls=%fused_computation.39 | custom fusion | bytes 2097664 | tf_op jit(solution)/shard_map/scatter | solution.py:144
  21.7 70.8 %all_to_all.20 = bf16[64,8,2048]{2,1,0:T(8,128)(2,1)S(1)} all-to-all(bf16[64,8,2048]{2,1,0:T(8,128)(2,1)S(1)} %bitcast.104), channel_id=1, replica_groups=mesh['ep'=64,'tp'=4] {'ep'}, dimensions={0} | all-to-all | bytes 4194304 | tf_op jit(solution)/shard_map/all_to_all | solution.py:146
  92.5 4.3 broadcast_in_dim.19
  96.8 5.8 %all-to-all-start.2 = ((bf16[4,64,8,2048]{3,2,1,0:T(8,128)(2,1)}), bf16[4,64,8,2048]{3,2,1,0:T(8,128)(2,1)}, u32[]{:S(2)}, u32[]{:S(2)}) async-start(bf16[4,64,8,2048]{3,2,1,0:T(8,128)(2,1)} %broadcast_in_dim.19), calls=%async_computation.2 | async-start | bytes 16777216 | tf_op jit(solution)/shard_map/all_to_all | solution.py:29
  103.0 90.9 %all-to-all-done.2 = bf16[4,64,8,2048]{3,2,1,0:T(8,128)(2,1)} async-done(((bf16[4,64,8,2048]{3,2,1,0:T(8,128)(2,1)}), bf16[4,64,8,2048]{3,2,1,0:T(8,128)(2,1)}, u32[]{:S(2)}, u32[]{:S(2)}) %all-to-all-start.2) | async-done | bytes 8388640 | tf_op jit(solution)/shard_map/all_to_all | solution.py:29
  193.8 7.1 %fusion.24 = f32[2048,256]{1,0:T(8,128)} fusion(bf16[2048,2048]{1,0:T(8,128)(2,1)} %bitcast.15, bf16[1,2048,256]{2,1,0:T(8,128)(2,1)S(1)} %copy-done.9), kind=kOutput, calls=%fused_computation.37 | convolution fusion | flops 2147483648 | bytes 11534336 | tf_op jit(solution)/shard_map/dot_general | solution.py:50
  201.0 16.8 %convolution_convert_fusion = bf16[2048,2048]{1,0:T(8,128)(2,1)} fusion(bf16[2048,2048]{1,0:T(8,128)(2,1)} %bitcast.15, f32[2048,256]{1,0:T(8,128)} %fusion.24, bf16[1,256,2048]{2,1,0:T(8,128)(2,1)S(1)} %copy-done, bf16[1,2048,256]{2,1,0:T(8,128)(2,1)} %param.28), kind=kOutput, calls=%fused_computation.25 | convolution fusion | flops 4302307328 | bytes 20971520 | tf_op jit(solution)/shard_map/dot_general | solution.py:158
  217.8 21.8 %reshape.281 = bf16[12,1024,2,2,64]{4,3,2,1,0:T(2,128)(2,1)} reshape(bf16[12288,256]{1,0:T(8,128)(2,1)} %all-gather.3.cloned.1.call-done) | data formatting | bytes 12582912 | tf_op jit(solution)/shard_map/reshape | solution.py:108
  239.6 29.7 %copy.37 = bf16[12,1024,2,2,64]{1,4,3,2,0:T(8,128)(2,1)} copy(bf16[12,1024,2,2,64]{4,3,2,1,0:T(2,128)(2,1)} %reshape.281) | data formatting | bytes 12582912
  269.3 9.8 %reshape.244 = bf16[12,1024,2,128]{3,2,1,0:T(2,128)(2,1)} reshape(bf16[12288,256]{1,0:T(8,128)(2,1)} %all-gather.5.cloned.1.call-done) | data formatting | bytes 12582912 | tf_op jit(solution)/shard_map/reshape | solution.py:109
  279.1 67.7 %while.15 = (s32[]{:T(128)}, f32[2,2,192]{2,1,0:T(2,128)S(1)}, f32[2,2,192]{2,1,0:T(2,128)S(1)}, f32[2,2,192,128]{3,2,1,0:T(8,128)}, bf16[12,1024,2,2,64]{1,4,3,...) while((s32[]{:T(128)}, f32[2,2,192]{2,1,0:T(2,128)S(1)}, ...), condition=%wide.region_3.4_spmd.clone, body=%wide.region_0.3_spmd.clone.sunk | while | flops 308580096 | bytes 15614629 | solution.py:111
  279.1 1.8 bitcast_reduce_fusion.2
  281.6 1.4 constant_dynamic-slice_fusion.6
  283.1 1.0 fusion.60
  284.0 0.7 copy-done.3
  284.8 1.7 bitcast_reduce_fusion.2
  287.3 1.4 constant_dynamic-slice_fusion.6
  288.7 1.0 fusion.60
  289.7 0.7 copy-done.3
  290.4 1.7 bitcast_reduce_fusion.2
  292.9 1.4 constant_dynamic-slice_fusion.6
  294.4 1.0 fusion.60
  295.3 0.7 copy-done.3
  296.1 1.7 bitcast_reduce_fusion.2
  298.6 1.4 constant_dynamic-slice_fusion.6
  300.0 1.0 fusion.60
  301.7 1.7 bitcast_reduce_fusion.2
  304.2 1.4 constant_dynamic-slice_fusion.6
  305.6 1.0 fusion.60
  306.6 0.7 copy-done.3
  307.4 1.7 bitcast_reduce_fusion.2
  309.9 1.4 constant_dynamic-slice_fusion.6
  311.3 1.0 fusion.60
  312.3 0.7 copy-done.3
  313.0 1.7 bitcast_reduce_fusion.2
  315.5 1.4 constant_dynamic-slice_fusion.6
  316.9 1.0 fusion.60
  317.9 0.7 copy-done.3
  318.6 1.7 bitcast_reduce_fusion.2
  321.1 1.4 constant_dynamic-slice_fusion.6
  322.6 1.0 fusion.60
  324.3 1.7 bitcast_reduce_fusion.2
  326.8 1.4 constant_dynamic-slice_fusion.6
  328.2 1.0 fusion.60
  329.9 1.7 bitcast_reduce_fusion.2
  332.4 1.4 constant_dynamic-slice_fusion.6
  333.8 1.0 fusion.60
  335.6 1.7 bitcast_reduce_fusion.2
  338.1 1.4 constant_dynamic-slice_fusion.6
  339.5 1.0 fusion.60
  341.2 1.7 bitcast_reduce_fusion.2
  343.7 1.4 constant_dynamic-slice_fusion.6
  345.1 1.0 fusion.60
  346.9 1.2 broadcast_divide_fusion
  348.3 1.7 convolution_convert_fusion.1
  350.0 11.1 %all_to_all.21 = bf16[4,48,2048]{2,1,0:T(8,128)(2,1)S(1)} all-to-all(bf16[4,48,2048]{2,1,0:T(8,128)(2,1)S(1)} %bitcast.106), channel_id=1, replica_groups=mesh['ep'=64,'tp'=4] {'tp'}, dimensions={0} | all-to-all | bytes 1572864 | tf_op jit(solution)/shard_map/all_to_all | solution.py:17
  361.1 15.1 %all-to-all-start.3 = ((bf16[64,8,2048]{2,1,0:T(8,128)(2,1)}), bf16[64,8,2048]{2,1,0:T(8,128)(2,1)S(1)}, u32[]{:S(2)}, u32[]{:S(2)}) async-start(bf16[64,8,2048]{2,1,0:T(8,128)(2,1)} %bitcast.107), calls=%async_computation.4 | async-start | bytes 4194304 | tf_op jit(solution)/shard_map/all_to_all | solution.py:163
  376.5 0.8 reduce_sum.87
  377.3 48.6 %all-to-all-done.3 = bf16[64,8,2048]{2,1,0:T(8,128)(2,1)S(1)} async-done(((bf16[64,8,2048]{2,1,0:T(8,128)(2,1)}), bf16[64,8,2048]{2,1,0:T(8,128)(2,1)S(1)}, u32[]{:S(2)}, u32[]{:S(2)}) %all-to-all-start.3) | async-done | bytes 2097184 | tf_op jit(solution)/shard_map/all_to_all | solution.py:163
  425.9 2.3 gather_fusion
  428.3 2.4 reshape.255
  430.6 3.9 multiply_reduce_fusion
  (151 shorter events, 18.2 us)
Async XLA Ops:
  8.0 193.0 %copy-start = (bf16[1,256,2048]{2,1,0:T(8,128)(2,1)S(1)}, bf16[1,256,2048]{2,1,0:T(8,128)(2,1)}, u32[]{:S(2)}) copy-start(bf16[1,256,2048]{2,1,0:T(8,128)(2,1)} %param.29) | copy-start | bytes 3145732
  8.0 209.7 %all-gather.3.cloned.1.call-start = ((), (), s32[]{:S(2)}) async-start(), calls=%async_computation.5 | async-start | bytes 6389760 | tf_op jit(solution)/shard_map/all_gather | solution.py:103
  8.7 260.6 %all-gather.5.cloned.1.call-start = ((), (), s32[]{:S(2)}) async-start(), calls=%async_computation.6 | async-start | bytes 6389760 | tf_op jit(solution)/shard_map/all_gather | solution.py:104
  96.8 6.1 %copy-start.4 = (bf16[192,256]{1,0:T(8,128)(2,1)S(1)}, bf16[192,256]{1,0:T(8,128)(2,1)}, u32[]{:S(2)}) copy-start(bf16[192,256]{1,0:T(8,128)(2,1)} %param.16) | copy-start | bytes 294916
  96.8 97.1 %copy-start.9 = (bf16[1,2048,256]{2,1,0:T(8,128)(2,1)S(1)}, bf16[1,2048,256]{2,1,0:T(8,128)(2,1)}, u32[]{:S(2)}) copy-start(bf16[1,2048,256]{2,1,0:T(8,128)(2,1)} %param.27) | copy-start | bytes 3145732
  96.8 97.0 %all-to-all-start.2 = ((bf16[4,64,8,2048]{3,2,1,0:T(8,128)(2,1)}), bf16[4,64,8,2048]{3,2,1,0:T(8,128)(2,1)}, u32[]{:S(2)}, u32[]{:S(2)}) async-start(bf16[4,64,8,2048]{3,2,1,0:T(8,128)(2,1)} %broadcast_in_dim.19), calls=%async_computation.2 | async-start | bytes 16777216 | tf_op jit(solution)/shard_map/all_to_all | solution.py:29
  102.6 258.5 %reduce-scatter.2.cloned.1.call-start = ((), (), s32[]{:S(2)}) async-start(), calls=%async_computation.7 | async-start | bytes 10485760 | tf_op jit(solution)/shard_map/reduce_scatter | solution.py:157
  279.1 68.9 %copy-start.7 = (f32[2]{0:T(128)S(1)}, f32[2]{0:T(128)}, u32[]{:S(2)}) copy-start(f32[2]{0:T(128)} %param.19) | copy-start | bytes 28
  279.1 69.2 %copy-start.8 = (f32[128]{0:T(128)S(1)}, f32[128]{0:T(128)}, u32[]{:S(2)}) copy-start(f32[128]{0:T(128)} %param.20) | copy-start | bytes 1540
  280.9 2.2 copy-start.2
  284.0 0.7 copy-start.3
  286.5 2.2 copy-start.2
  289.7 0.7 copy-start.3
  292.2 2.2 copy-start.2
  295.3 0.7 copy-start.3
  297.8 2.2 copy-start.2
  301.0 0.7 copy-start.3
  303.5 2.2 copy-start.2
  306.6 0.7 copy-start.3
  309.1 2.2 copy-start.2
  312.3 0.7 copy-start.3
  314.8 2.2 copy-start.2
  317.9 0.7 copy-start.3
  320.4 2.2 copy-start.2
  323.5 0.7 copy-start.3
  326.0 2.2 copy-start.2
  329.2 0.7 copy-start.3
  331.7 2.2 copy-start.2
  334.8 0.7 copy-start.3
  337.3 2.2 copy-start.2
  340.5 0.7 copy-start.3
  343.0 2.2 copy-start.2
  346.1 0.7 copy-start.3
  350.0 26.3 %copy-start.5 = (f32[512,4]{0,1:T(4,128)S(1)}, f32[512,4]{0,1:T(4,128)}, u32[]{:S(2)}) copy-start(f32[512,4]{0,1:T(4,128)} %param.25) | copy-start | bytes 24580
  350.0 26.3 %copy-start.6 = (f32[512,2]{0,1:T(2,128)S(1)}, f32[512,2]{0,1:T(2,128)}, u32[]{:S(2)}) copy-start(f32[512,2]{0,1:T(2,128)} %param.26) | copy-start | bytes 12292
  361.1 64.8 %all-to-all-start.3 = ((bf16[64,8,2048]{2,1,0:T(8,128)(2,1)}), bf16[64,8,2048]{2,1,0:T(8,128)(2,1)S(1)}, u32[]{:S(2)}, u32[]{:S(2)}) async-start(bf16[64,8,2048]{2,1,0:T(8,128)(2,1)} %bitcast.107), calls=%async_computation.4 | async-start | bytes 4194304 | tf_op jit(solution)/shard_map/all_to_all | solution.py:163
  425.9 8.7 %copy-start.1 = (bf16[1,256,2048]{2,1,0:T(8,128)(2,1)S(1)}, bf16[1,256,2048]{2,1,0:T(8,128)(2,1)}, u32[]{:S(2)}) copy-start(bf16[1,256,2048]{2,1,0:T(8,128)(2,1)} %param.29) | copy-start | bytes 3145732
Sparse Core Ops, SparseCore 0:
  11.6 96.1 all-gather.2
  110.6 78.3 all-gather.4
Sparse Core Ops, SparseCore 1:
  217.8 83.4 reduce-scatter.1
where the time goes:
time: 445 us; the launch traced here: 442 us
  waiting for transfers between devices  141 us (32%)
  local copies, waits for them, and re-layouts  104 us (23%)
  blocking collectives  81.9 us (18%)
  matrix products  58.1 us (13%)
  starting transfers between devices  21.2 us (5%)
  other arithmetic  19.7 us (4%)
  between operations  15.7 us (4%)
    all_to_all x1, waiting for transfers between devices, copy_for_each(): lax.all_to_all(jnp.broadcast_to(x[None], (peers, *x.shape)), axis, 0, 0,...  90.9 us
    all_to_all x1, blocking collectives, local(): lax.all_to_all(outgoing.reshape(expert_count, capacity, model_width), 'ep...  70.8 us
    all_to_all x1, waiting for transfers between devices, local(): lax.all_to_all(summed.reshape(expert_count, capacity, model_width), 'ep',...  48.6 us
    unnamed x18, local copies, waits for them, and re-layouts  29.9 us
    reshape x1, local copies, waits for them, and re-layouts, local(): key_piece.reshape(length // block_rows, block_rows, local_heads, 2, head_qk)  21.8 us
    dot_general x12, matrix products, absorb(): jnp.einsum('qhmd,khmd->hmqk', queries, key_block, preferred_element_type=...  20.9 us
    dynamic_slice x12, local copies, waits for them, and re-layouts, local(): carried, unused = lax.scan(absorb, carried, blocks)  16.9 us
    dot_general x1, matrix products, local(): jnp.dot(hidden_flat, w_down[0], preferred_element_type=jnp.float32)  16.8 us
  transfers between devices with their start and end apart: 5, of which 2 were waited for; matrix products, arithmetic and copies ran while one was open for 37% of the time, Pallas kernels for 0%

commit v1 on v0

v1 whole, which is shorter than its diff:
```python
import jax
import jax.numpy as jnp
from jax import lax
from jax.experimental import pallas as pl
from jax.experimental.pallas import tpu as pltpu
from jax.sharding import PartitionSpec as P

EPS = 1e-06
HEAD_SCALE = 0.8
NZ, NXC, NT = 8, 8, 4
CAP = 8
EXPERTS = 64
ROWS = 192
TOK = 128
D = 2048
HALF = D // 2
UNITS = 256
SLOTS = EXPERTS * CAP
Z_ORDER = (1, 7, 2, 6, 3, 5, 4)
F32 = jnp.float32
BF16 = jnp.bfloat16
MESH = pl.DeviceIdType.MESH


def dot(a, b):
    return lax.dot_general(a, b, (((1,), (0,)), ((), ())), preferred_element_type=F32)


def kernel(
    q_hbm,
    k_hbm,
    v_hbm,
    lam_ref,
    hg_ref,
    wo_hbm,
    moe_hbm,
    fg_ref,
    routes_ref,
    gl_ref,
    pk_ref,
    wg_hbm,
    wu_hbm,
    wd_hbm,
    mix_ref,
    moe_ref,
    qbuf,
    kbuf,
    vbuf,
    psend,
    precv,
    att,
    attall,
    wob,
    xin,
    gmat,
    dsend,
    dmid,
    dout,
    wgb,
    wub,
    wdb,
    hid,
    osend,
    omid,
    oret,
    loc_sem,
    q_ss,
    q_rs,
    k_ss,
    k_rs,
    v_ss,
    v_rs,
    p_ss,
    p_rs,
    a_ss,
    a_rs,
    w_ss,
    w_rs,
    f_ss,
    f_rs,
    d1_ss,
    d1_rs,
    d2_ss,
    d2_rs,
    o1_ss,
    o1_rs,
    o2_ss,
    o2_rs,
):
    ep = lax.axis_index("ep")
    t = lax.axis_index("tp")
    z = ep // NXC
    xc = ep % NXC

    def z_peer(k):
        return ((z + k) % NZ) * NXC + xc

    def xc_peer(j):
        return z * NXC + (xc + j) % NXC

    def remote(src, dst, ssem, rsem, to_ep, to_tp):
        return pltpu.make_async_remote_copy(
            src_ref=src,
            dst_ref=dst,
            send_sem=ssem,
            recv_sem=rsem,
            device_id=(to_ep, to_tp),
            device_id_type=MESH,
        )

    locals_ = [
        (moe_hbm.at[pl.ds(pl.multiple_of(t * TOK, TOK), TOK)], xin),
        (q_hbm, qbuf.at[xc]),
        (k_hbm, kbuf.at[z]),
        (v_hbm, vbuf.at[z]),
        (wg_hbm.at[0], wgb.at[t]),
        (wu_hbm.at[0], wub.at[t]),
        (wd_hbm.at[0, :, pl.ds(0, HALF)], wdb.at[0, t]),
        (wd_hbm.at[0, :, pl.ds(HALF, HALF)], wdb.at[1, t]),
        (wo_hbm, wob),
    ]
    loads = [
        pltpu.make_async_copy(src, dst, loc_sem.at[i]) for i, (src, dst) in enumerate(locals_)
    ]
    for load in loads:
        load.start()

    barrier = pltpu.get_barrier_semaphore()
    for k in range(1, NZ):
        pl.semaphore_signal(barrier, inc=1, device_id=(z_peer(k), t), device_id_type=MESH)
    for j in range(1, NXC):
        pl.semaphore_signal(barrier, inc=1, device_id=(xc_peer(j), t), device_id_type=MESH)
    for y in range(1, NT):
        pl.semaphore_signal(barrier, inc=1, device_id=(ep, (t + y) % NT), device_id_type=MESH)
    pl.semaphore_wait(barrier, NZ - 1 + NXC - 1 + NT - 1)

    right = (t + 1) % NT
    left = (t + 3) % NT

    def w_piece(owner, piece, half=None):
        if piece < 2:
            buf = wgb if piece == 0 else wub
            if half is None:
                return buf.at[owner]
            return buf.at[owner, pl.ds(half * HALF, HALF)]
        if half is None:
            return wdb.at[piece - 2, owner]
        return wdb.at[piece - 2, owner, pl.ds(half * (UNITS // 2), UNITS // 2)]

    def w_source(piece):
        if piece == 0:
            return wg_hbm.at[0]
        if piece == 1:
            return wu_hbm.at[0]
        return wd_hbm.at[0, :, pl.ds((piece - 2) * HALF, HALF)]

    def w_own(way, piece):
        to = right if way == 0 else left
        return remote(
            w_source(piece),
            w_piece(t, piece),
            w_ss.at[way * 4 + piece],
            w_rs.at[way * 4 + piece],
            ep,
            to,
        )

    def w_forward(way, piece):
        owner = left if way == 0 else right
        to = right if way == 0 else left
        return remote(
            w_piece(owner, piece, way),
            w_piece(owner, piece, way),
            f_ss.at[way * 4 + piece],
            f_rs.at[way * 4 + piece],
            ep,
            to,
        )

    def forward_piece(piece):
        for way in range(2):
            w_own(way, piece).wait_recv()
            w_forward(way, piece).start()

    for piece in range(2):
        for way in range(2):
            w_own(way, piece).start()

    def q_copy(j):
        return remote(q_hbm, qbuf.at[xc], q_ss.at[j], q_rs.at[j], xc_peer(j), t)

    def k_copy(k):
        return remote(k_hbm, kbuf.at[z], k_ss.at[k], k_rs.at[k], z_peer(k), t)

    def v_copy(k):
        return remote(v_hbm, vbuf.at[z], v_ss.at[k], v_rs.at[k], z_peer(k), t)

    for j in range(1, NXC):
        q_copy(j).start()
    for k in Z_ORDER:
        k_copy(k).start()
        v_copy(k).start()

    base = pl.multiple_of(t * TOK, TOK)
    picks = routes_ref[pl.ds(base, TOK), :]
    expert_iota = lax.broadcasted_iota(jnp.int32, (TOK, EXPERTS), 1)
    one0 = (picks[:, 0:1] == expert_iota).astype(F32)
    one1 = (picks[:, 1:2] == expert_iota).astype(F32)
    lower = (
        lax.broadcasted_iota(jnp.int32, (TOK, TOK), 1)
        < lax.broadcasted_iota(jnp.int32, (TOK, TOK), 0)
    ).astype(BF16)
    before0 = dot(lower, one0.astype(BF16))
    before1 = dot(lower, one1.astype(BF16)) + jnp.sum(one0, axis=0, keepdims=True)
    rank0 = jnp.sum(before0 * one0, axis=1, keepdims=True)
    rank1 = jnp.sum(before1 * one1, axis=1, keepdims=True)
    slot0 = picks[:, 0:1] * CAP + rank0.astype(jnp.int32)
    slot1 = picks[:, 1:2] * CAP + rank1.astype(jnp.int32)
    slot_iota = lax.broadcasted_iota(jnp.int32, (TOK, SLOTS), 1)
    hit0 = slot_iota == slot0
    hit1 = slot_iota == slot1

    groups = gl_ref[pl.ds(base, TOK), :]
    group_exp = jnp.exp(groups - jnp.max(groups, axis=1, keepdims=True))
    group_prob = group_exp / jnp.sum(group_exp, axis=1, keepdims=True)
    group_iota = lax.broadcasted_iota(jnp.int32, (TOK, 4), 1)
    share0 = jnp.sum(jnp.where((picks[:, 0:1] >> 4) == group_iota, group_prob, 0.0), axis=1, keepdims=True)
    share1 = jnp.sum(jnp.where((picks[:, 1:2] >> 4) == group_iota, group_prob, 0.0), axis=1, keepdims=True)
    pick_logits = pk_ref[pl.ds(base, TOK), :]
    pick_exp = jnp.exp(pick_logits - jnp.max(pick_logits, axis=1, keepdims=True))
    pick_prob = pick_exp / jnp.sum(pick_exp, axis=1, keepdims=True)
    gate0 = share0 * pick_prob[:, 0:1]
    gate1 = share1 * pick_prob[:, 1:2]
    gmat[...] = jnp.where(hit0, gate0, 0.0) + jnp.where(hit1, gate1, 0.0)

    spread = (hit0 | hit1).astype(F32).T.astype(BF16)
    loads[0].wait()
    rows = xin[...].astype(F32)
    squared = jnp.mean(rows * rows, axis=1, keepdims=True)
    xin[...] = (rows * lax.rsqrt(squared + EPS) * fg_ref[...]).astype(BF16)
    for c in range(4):
        cols = pl.ds(c * 512, 512)
        laid = dot(spread, xin[:, cols])
        dsend[:, :, cols] = laid.reshape(EXPERTS, CAP, 512).astype(BF16)

    def d1_copy(k):
        return remote(
            dsend.at[pl.ds(((z + k) % NZ) * NXC, NXC)],
            dmid.at[pl.ds(z * NXC, NXC)],
            d1_ss.at[k],
            d1_rs.at[k],
            z_peer(k),
            t,
        )

    def d2_copy(k, j):
        zs = (z + NZ - k) % NZ
        return remote(
            dmid.at[zs * NXC + (xc + j) % NXC],
            dout.at[zs * NXC + xc],
            d2_ss.at[k * NXC + j],
            d2_rs.at[k * NXC + j],
            xc_peer(j),
            t,
        )

    def o1_copy(h, k):
        return remote(
            osend.at[h, pl.ds(((z + k) % NZ) * NXC, NXC)],
            omid.at[h, pl.ds(z * NXC, NXC)],
            o1_ss.at[h * NZ + k],
            o1_rs.at[h * NZ + k],
            z_peer(k),
            t,
        )

    def o2_copy(h, k, j):
        zs = (z + NZ - k) % NZ
        return remote(
            omid.at[h, zs * NXC + (xc + j) % NXC],
            oret.at[h, zs * NXC + xc],
            o2_ss.at[h * 64 + k * NXC + j],
            o2_rs.at[h * 64 + k * NXC + j],
            xc_peer(j),
            t,
        )

    for k in Z_ORDER:
        d1_copy(k).start()
    dmid[pl.ds(z * NXC, NXC)] = dsend[pl.ds(z * NXC, NXC)]

    def d2_stage(k):
        @pl.loop(1, NXC)
        def _(j):
            d2_copy(k, j).start()

        zs = (z + NZ - k) % NZ
        dout[zs * NXC + xc] = dmid[zs * NXC + xc]

    d2_stage(0)

    forward_piece(0)

    for load in loads[1:4]:
        load.wait()
    for j in range(1, NXC):
        q_copy(j).wait_recv()
    for k in Z_ORDER:
        k_copy(k).wait_recv()
        v_copy(k).wait_recv()

    lane = lax.broadcasted_iota(jnp.int32, (ROWS, 128), 1)

    def p_copy(j):
        return remote(
            psend.at[(xc + j) % NXC], precv.at[xc], p_ss.at[j], p_rs.at[j], xc_peer(j), t
        )

    def attend(j, dst):
        source = (xc + j) % NXC
        stats = jnp.zeros((ROWS, 128), F32)
        for h in range(2):
            cols = pl.ds(h * 128, 128)
            query = qbuf[source, :, cols].astype(F32) * 0.125
            keys = kbuf[:, :, cols].reshape(NZ * ROWS, 128)
            values = vbuf[:, :, cols].reshape(NZ * ROWS, 128)
            for m in range(2):
                own = (lane >= 64) if m else (lane < 64)
                masked = jnp.where(own, query, 0.0).astype(BF16)
                scores = lax.dot_general(
                    masked, keys, (((1,), (1,)), ((), ())), preferred_element_type=F32
                )
                top = jnp.max(scores, axis=1, keepdims=True)
                weights = jnp.exp(scores - top)
                total = jnp.sum(weights, axis=1, keepdims=True)
                summed = dot(weights.astype(BF16), values)
                i = h * 2 + m
                dst[:, pl.ds(i * 128, 128)] = (summed / total).astype(BF16)
                lse = top + jnp.log(total)
                high = lse.astype(BF16).astype(F32)
                mid = (lse - high).astype(BF16).astype(F32)
                low = lse - high - mid
                stats = jnp.where(lane == i, high, stats)
                stats = jnp.where(lane == 4 + i, mid, stats)
                stats = jnp.where(lane == 8 + i, low, stats)
        dst[:, pl.ds(512, 128)] = stats.astype(BF16)

    @pl.loop(1, 5)
    def _(j):
        attend(j, psend.at[(xc + j) % NXC])
        p_copy(j).start()

    forward_piece(1)
    for way in range(2):
        w_own(way, 2).start()

    @pl.loop(5, NXC)
    def _(j):
        attend(j, psend.at[(xc + j) % NXC])
        p_copy(j).start()

    attend(0, precv.at[xc])

    for way in range(2):
        w_own(way, 3).start()

    for k in Z_ORDER:
        d1_copy(k).wait_recv()
        d2_stage(k)

    for j in range(1, NXC):
        p_copy(j).wait_recv()
    lses = []
    for d in range(NXC):
        stats = precv[d, :, pl.ds(512, 128)].astype(F32)
        lses.append(stats + pltpu.roll(stats, 124, 1) + pltpu.roll(stats, 120, 1))
    highest = lses[0]
    for d in range(1, NXC):
        highest = jnp.maximum(highest, lses[d])
    shares = [jnp.exp(lses[d] - highest) for d in range(NXC)]
    whole = shares[0]
    for d in range(1, NXC):
        whole = whole + shares[d]
    for d in range(NXC):
        shares[d] = shares[d] / whole
    for h in range(2):
        mixed = []
        for m in range(2):
            i = h * 2 + m
            acc = jnp.zeros((ROWS, 128), F32)
            for d in range(NXC):
                acc = acc + shares[d][:, i : i + 1] * precv[d, :, pl.ds(i * 128, 128)].astype(F32)
            mixed.append(acc)
        per_head = mixed[0] - lam_ref[h] * mixed[1]
        squared = jnp.mean(per_head * per_head, axis=1, keepdims=True)
        normed = per_head * lax.rsqrt(squared + EPS) * hg_ref[...] * HEAD_SCALE
        for y in range(NT):
            att[y, :, pl.ds(h * 128, 128)] = normed[y * 48 : (y + 1) * 48].astype(BF16)

    def a_copy(y):
        return remote(
            att.at[(t + y) % NT], attall.at[t], a_ss.at[y], a_rs.at[y], ep, (t + y) % NT
        )

    for y in range(1, NT):
        a_copy(y).start()
    attall[t] = att[t]

    forward_piece(2)

    @pl.loop(1, NXC)
    def _(j):
        for k in range(NZ):
            d2_copy(k, j).wait_recv()

    for load in loads[4:6]:
        load.wait()
    for piece in range(2):
        for way in range(2):
            w_forward(way, piece).wait_recv()

    @pl.loop(0, 2)
    def _(r):
        arrived = dout[pl.ds(r * 32, 32)].astype(F32).reshape(256, D).astype(BF16)
        for b in range(NT):
            gate_part = dot(arrived, wgb[b])
            up_part = dot(arrived, wub[b])
            hidden = gate_part / (1.0 + jnp.exp(-gate_part)) * up_part
            hid[pl.ds(pl.multiple_of(r * 256, 256), 256), pl.ds(b * UNITS, UNITS)] = hidden.astype(BF16)

    forward_piece(3)

    def down(h):
        loads[6 + h].wait()
        for way in range(2):
            w_forward(way, 2 + h).wait_recv()

        @pl.loop(0, 2)
        def _(r):
            part = hid[pl.ds(pl.multiple_of(r * 256, 256), 256), :]
            for c in range(2):
                cols = pl.ds(c * 512, 512)
                result = dot(part, wdb[h, :, :, cols].reshape(NT * UNITS, 512))
                osend[h, pl.ds(r * 32, 32), :, cols] = result.reshape(32, CAP, 512).astype(BF16)

        for k in Z_ORDER:
            o1_copy(h, k).start()
        omid[h, pl.ds(z * NXC, NXC)] = osend[h, pl.ds(z * NXC, NXC)]

    def o2_stage(h, k):
        @pl.loop(1, NXC)
        def _(j):
            o2_copy(h, k, j).start()

        zs = (z + NZ - k) % NZ
        oret[h, zs * NXC + xc] = omid[h, zs * NXC + xc]

    down(0)
    o2_stage(0, 0)
    down(1)
    o2_stage(1, 0)

    loads[8].wait()
    for y in range(1, NT):
        a_copy(y).wait_recv()
    for c in range(4):
        cols = pl.ds(c * 512, 512)
        acc = dot(attall[0], wob[pl.ds(0, 256), cols])
        for y in range(1, NT):
            acc = acc + dot(attall[y], wob[pl.ds(y * 256, 256), cols])
        mix_ref[:, cols] = acc.astype(BF16)

    for h in range(2):
        for k in Z_ORDER:
            o1_copy(h, k).wait_recv()
            o2_stage(h, k)

    gates = gmat[...]
    gates_high = gates.astype(BF16)
    gates_low = (gates - gates_high.astype(F32)).astype(BF16)
    for h in range(2):

        @pl.loop(1, NXC)
        def _(j):
            for k in range(NZ):
                o2_copy(h, k, j).wait_recv()

        for c in range(2):
            returned = oret[h, :, :, pl.ds(c * 512, 512)].astype(F32).reshape(SLOTS, 512).astype(BF16)
            result = dot(gates_high, returned) + dot(gates_low, returned)
            moe_ref[:, pl.ds(h * HALF + c * 512, 512)] = result.astype(BF16)

    for j in range(1, NXC):
        q_copy(j).wait_send()
        p_copy(j).wait_send()
    for k in range(1, NZ):
        k_copy(k).wait_send()
        v_copy(k).wait_send()
        d1_copy(k).wait_send()
        for h in range(2):
            o1_copy(h, k).wait_send()
    for y in range(1, NT):
        a_copy(y).wait_send()
    for way in range(2):
        for piece in range(4):
            w_own(way, piece).wait_send()
            w_forward(way, piece).wait_send()

    @pl.loop(1, NXC)
    def _(j):
        for k in range(NZ):
            d2_copy(k, j).wait_send()
            for h in range(2):
                o2_copy(h, k, j).wait_send()


def local(
    query_rows,
    key_rows,
    value_rows,
    lambdas,
    head_gain,
    w_out,
    moe_rows,
    ffn_gain,
    routes,
    group_logits,
    pick_logits,
    w_gate,
    w_up,
    w_down,
):
    any_ = pl.BlockSpec(memory_space=pl.ANY)
    vmem = pl.BlockSpec(memory_space=pltpu.VMEM)
    smem = pl.BlockSpec(memory_space=pltpu.SMEM)
    dma = pltpu.SemaphoreType.DMA
    return pl.pallas_call(
        kernel,
        out_shape=(
            jax.ShapeDtypeStruct((ROWS // NT, D), BF16),
            jax.ShapeDtypeStruct((TOK, D), BF16),
        ),
        in_specs=[any_, any_, any_, smem, vmem, any_, any_, vmem, vmem, vmem, vmem, any_, any_, any_],
        out_specs=(vmem, vmem),
        scratch_shapes=[
            pltpu.VMEM((NXC, ROWS, 256), BF16),
            pltpu.VMEM((NZ, ROWS, 256), BF16),
            pltpu.VMEM((NZ, ROWS, 256), BF16),
            pltpu.VMEM((NXC, ROWS, 640), BF16),
            pltpu.VMEM((NXC, ROWS, 640), BF16),
            pltpu.VMEM((NT, 48, 256), BF16),
            pltpu.VMEM((NT, 48, 256), BF16),
            pltpu.VMEM((1024, D), BF16),
            pltpu.VMEM((TOK, D), BF16),
            pltpu.VMEM((TOK, SLOTS), F32),
            pltpu.VMEM((EXPERTS, CAP, D), BF16),
            pltpu.VMEM((EXPERTS, CAP, D), BF16),
            pltpu.VMEM((EXPERTS, CAP, D), BF16),
            pltpu.VMEM((NT, D, UNITS), BF16),
            pltpu.VMEM((NT, D, UNITS), BF16),
            pltpu.VMEM((2, NT, UNITS, HALF), BF16),
            pltpu.VMEM((SLOTS, 1024), BF16),
            pltpu.VMEM((2, EXPERTS, CAP, HALF), BF16),
            pltpu.VMEM((2, EXPERTS, CAP, HALF), BF16),
            pltpu.VMEM((2, EXPERTS, CAP, HALF), BF16),
            dma((9,)),
            dma((NXC,)),
            dma((NXC,)),
            dma((NZ,)),
            dma((NZ,)),
            dma((NZ,)),
            dma((NZ,)),
            dma((NXC,)),
            dma((NXC,)),
            dma((NT,)),
            dma((NT,)),
            dma((8,)),
            dma((8,)),
            dma((8,)),
            dma((8,)),
            dma((NZ,)),
            dma((NZ,)),
            dma((64,)),
            dma((64,)),
            dma((2 * NZ,)),
            dma((2 * NZ,)),
            dma((128,)),
            dma((128,)),
        ],
        compiler_params=pltpu.CompilerParams(
            collective_id=0, has_side_effects=True, vmem_limit_bytes=66_000_000
        ),
    )(
        query_rows,
        key_rows,
        value_rows,
        lambdas,
        head_gain[None],
        w_out,
        moe_rows,
        ffn_gain[None],
        routes,
        group_logits,
        pick_logits,
        w_gate,
        w_up,
        w_down,
    )


def solution(mesh):
    return jax.shard_map(
        local,
        mesh=mesh,
        in_specs=(
            P("ep", "tp"),
            P("ep", "tp"),
            P("ep", "tp"),
            P("tp"),
            P(),
            P(),
            P("ep", None),
            P(),
            P("ep", None),
            P("ep", None),
            P("ep", None),
            P("ep", None, "tp"),
            P("ep", None, "tp"),
            P("ep", "tp", None),
        ),
        out_specs=(P(("ep", "tp"), None), P(("ep", "tp"), None)),
        check_vma=False,
    )
```

time: 445 us -> 178 us (0.40)
  Pallas kernels: 0 us -> 169 us
  waiting for transfers between devices: 141 us -> 0 us
  local copies, waits for them, and re-layouts: 104 us -> 8.12 us
  blocking collectives: 81.9 us -> 0 us
  matrix products: 58.1 us -> 0 us
  starting transfers between devices: 21.2 us -> 0 us
  other arithmetic: 19.7 us -> 0 us
  between operations: 15.7 us -> 0.64 us
    pallas_call x0 -> x1, Pallas kernels: none -> 169 us  [local(): pl.pallas_call(kernel, out_shape=(jax.ShapeDtypeStruct((ROWS // NT, D), B...]
    all_to_all x2 -> x0, waiting for transfers between devices: 139 us -> none  [the longest x1 90.9 us: copy_for_each(): lax.all_to_all(jnp.broadcast_to(x[None], (peers, *x.shape)), axis, 0, 0,...]
    all_to_all x2 -> x0, blocking collectives: 81.9 us -> none  [the longest x1 70.8 us: local(): lax.all_to_all(outgoing.reshape(expert_count, capacity, model_width), 'ep...]
    dot_general x27 -> x0, matrix products: 58.1 us -> none  [the longest x12 20.9 us: absorb(): jnp.einsum('qhmd,khmd->hmqk', queries, key_block, preferred_element_type=...]
    reshape x4 -> x0, local copies, waits for them, and re-layouts: 31.7 us -> none  [the longest x1 21.8 us: local(): key_piece.reshape(length // block_rows, block_rows, local_heads, 2, head_qk)]
    unnamed x18 -> x5, local copies, waits for them, and re-layouts: 29.9 us -> 8.12 us
    all_to_all x2 -> x0, starting transfers between devices: 20.9 us -> none  [the longest x1 15.1 us: local(): lax.all_to_all(summed.reshape(expert_count, capacity, model_width), 'ep',...]
    dynamic_slice x13 -> x0, local copies, waits for them, and re-layouts: 17 us -> none  [the longest x12 16.9 us: local(): carried, unused = lax.scan(absorb, carried, blocks)]
  transfers between devices with their start and end apart: 5 -> 0, of which waited for: 2 -> 0; matrix products, arithmetic and copies ran while one was open for 37% -> 0% of each run, Pallas kernels for 0% -> 0%
where the time goes in v1:
time: 178 us
  Pallas kernels  169 us (95%)
  local copies, waits for them, and re-layouts  8.12 us (5%)
    pallas_call x1, Pallas kernels, local(): pl.pallas_call(kernel, out_shape=(jax.ShapeDtypeStruct((ROWS // NT, D), B...  169 us
    unnamed x5, local copies, waits for them, and re-layouts  8.12 us

profile of v1, /device:TPU:1, one launch (start us, length us, event | category | flops | bytes accessed | tf_op | source)
XLA Modules:
  0.0 178.0 jit_solution(11100821214915713203)
XLA Ops:
  0.6 1.5 copy.16.routes_ref
  2.2 1.5 copy.17.gl_ref
  3.7 1.5 copy.18.pk_ref
  5.3 169.2 %shard_map.149 = (bf16[48,2048]{1,0:T(8,128)(2,1)}, bf16[128,2048]{1,0:T(8,128)(2,1)}) custom-call(bf16[192,256]{1,0:T(8,128)(2,1)} %q_hbm.1, bf16[192,256]{1,0:T(8,128)(2,1)} %k_hbm.1, bf16[192,256]{1,0:T(8,128)(2,1)} %v_hbm.1, f32[2]{0:T(128)} %lam_ref.1, f32[1,128]{1,0:T(1,128)} %bitcast.3, bf16[1024,2048]{1,0:T(8,128)(2,1)} %wo_hbm.1, ...), custom_call_target="tpu_custom_call" | custom-call | tf_op jit(solution)/shard_map/pallas_call | solution.py:537
  174.5 1.6 copy.21
  176.1 1.9 %copy.22 = bf16[128,2048]{1,0:T(8,128)(2,1)} copy(bf16[128,2048]{1,0:T(8,128)(2,1)} %get-tuple-element.5) | data formatting | bytes 1048576

commit v2 on v1

v2 whole, which is shorter than its diff:
```python
import jax
import jax.numpy as jnp
from jax import lax
from jax.experimental import pallas as pl
from jax.experimental.pallas import tpu as pltpu
from jax.sharding import PartitionSpec as P

EPS = 1e-06
HEAD_SCALE = 0.8
NZ, NXC, NT = 8, 8, 4
CAP = 8
EXPERTS = 64
ROWS = 192
TOK = 128
D = 2048
HALF = D // 2
NCH = 8
CW = D // NCH
UNITS = 256
SLOTS = EXPERTS * CAP
Z_ORDER = (1, 7, 2, 6, 3, 5, 4)
F32 = jnp.float32
BF16 = jnp.bfloat16
MESH = pl.DeviceIdType.MESH


def dot(a, b):
    return lax.dot_general(a, b, (((1,), (0,)), ((), ())), preferred_element_type=F32)


def kernel(
    q_hbm,
    k_hbm,
    v_hbm,
    lam_ref,
    hg_ref,
    wo_hbm,
    moe_hbm,
    fg_ref,
    routes_ref,
    gl_ref,
    pk_ref,
    wg_hbm,
    wu_hbm,
    wd_hbm,
    mix_ref,
    moe_ref,
    qbuf,
    kbuf,
    vbuf,
    psend,
    precv,
    att,
    attall,
    wob,
    xin,
    gmat,
    dsend,
    dmid,
    dout,
    xall,
    wgb,
    wub,
    wdb,
    hid,
    osend,
    omid,
    oret,
    loc_sem,
    q_ss,
    q_rs,
    kv_ss,
    kv_rs,
    p_ss,
    p_rs,
    a_ss,
    a_rs,
    w_ss,
    w_rs,
    f_ss,
    f_rs,
    d1_ss,
    d1_rs,
    d2_ss,
    d2_rs,
    o1_ss,
    o1_rs,
    o2_ss,
    o2_rs,
):
    ep = lax.axis_index("ep")
    t = lax.axis_index("tp")
    z = ep // NXC
    xc = ep % NXC

    def z_peer(k):
        return ((z + k) % NZ) * NXC + xc

    def xc_peer(j):
        return z * NXC + (xc + j) % NXC

    def remote(src, dst, ssem, rsem, to_ep, to_tp):
        return pltpu.make_async_remote_copy(
            src_ref=src,
            dst_ref=dst,
            send_sem=ssem,
            recv_sem=rsem,
            device_id=(to_ep, to_tp),
            device_id_type=MESH,
        )
    base = pl.multiple_of(t * TOK, TOK)
    locals_ = [
        (moe_hbm.at[pl.ds(base, TOK)], xin),
        (q_hbm, qbuf.at[xc]),
        (k_hbm, kbuf.at[z]),
        (v_hbm, vbuf.at[z]),
        (wg_hbm.at[0], wgb.at[t]),
        (wu_hbm.at[0], wub.at[t]),
        (wo_hbm, wob),
    ] + [(wd_hbm.at[0, :, pl.ds(h * CW, CW)], wdb.at[h, t]) for h in range(NCH)]
    loads = [
        pltpu.make_async_copy(src, dst, loc_sem.at[i]) for i, (src, dst) in enumerate(locals_)
    ]
    for load in loads:
        load.start()

    barrier = pltpu.get_barrier_semaphore()
    for k in range(1, NZ):
        pl.semaphore_signal(barrier, inc=1, device_id=(z_peer(k), t), device_id_type=MESH)
    for j in range(1, NXC):
        pl.semaphore_signal(barrier, inc=1, device_id=(xc_peer(j), t), device_id_type=MESH)
    for y in range(1, NT):
        pl.semaphore_signal(barrier, inc=1, device_id=(ep, (t + y) % NT), device_id_type=MESH)
    mine = pl.ds(base, TOK)
    pick0 = routes_ref[0:1, mine]
    pick1 = routes_ref[1:2, mine]
    expert_iota = lax.broadcasted_iota(jnp.int32, (EXPERTS, TOK), 0)
    one0 = (pick0 == expert_iota).astype(F32)
    one1 = (pick1 == expert_iota).astype(F32)
    earlier = (
        lax.broadcasted_iota(jnp.int32, (TOK, TOK), 0)
        < lax.broadcasted_iota(jnp.int32, (TOK, TOK), 1)
    ).astype(BF16)
    before0 = dot(one0.astype(BF16), earlier)
    before1 = dot(one1.astype(BF16), earlier) + jnp.sum(one0, axis=1, keepdims=True)
    rank0 = jnp.sum(before0 * one0, axis=0, keepdims=True)
    rank1 = jnp.sum(before1 * one1, axis=0, keepdims=True)
    slot_iota = lax.broadcasted_iota(jnp.int32, (SLOTS, TOK), 0)
    hit0 = slot_iota == pick0 * CAP + rank0.astype(jnp.int32)
    hit1 = slot_iota == pick1 * CAP + rank1.astype(jnp.int32)

    spread = (hit0 | hit1).astype(F32).astype(BF16)
    loads[0].wait()
    rows = xin[...].astype(F32)
    squared = jnp.mean(rows * rows, axis=1, keepdims=True)
    xin[...] = (rows * lax.rsqrt(squared + EPS) * fg_ref[...]).astype(BF16)
    for c in range(4):
        cols = pl.ds(c * 512, 512)
        laid = dot(spread, xin[:, cols])
        dsend[:, :, cols] = laid.reshape(EXPERTS, CAP, 512).astype(BF16)

    groups = gl_ref[:, mine]
    group_exp = jnp.exp(groups - jnp.max(groups, axis=0, keepdims=True))
    group_prob = group_exp / jnp.sum(group_exp, axis=0, keepdims=True)
    group_iota = lax.broadcasted_iota(jnp.int32, (4, TOK), 0)
    share0 = jnp.sum(jnp.where((pick0 >> 4) == group_iota, group_prob, 0.0), axis=0, keepdims=True)
    share1 = jnp.sum(jnp.where((pick1 >> 4) == group_iota, group_prob, 0.0), axis=0, keepdims=True)
    pick_logits = pk_ref[:, mine]
    pick_exp = jnp.exp(pick_logits - jnp.max(pick_logits, axis=0, keepdims=True))
    pick_prob = pick_exp / jnp.sum(pick_exp, axis=0, keepdims=True)
    gate0 = share0 * pick_prob[0:1]
    gate1 = share1 * pick_prob[1:2]
    gates = (jnp.where(hit0, gate0, 0.0) + jnp.where(hit1, gate1, 0.0)).T
    gates_high = gates.astype(BF16)
    gmat[pl.ds(0, TOK), :] = gates_high
    gmat[pl.ds(TOK, TOK), :] = (gates - gates_high.astype(F32)).astype(BF16)
    pl.semaphore_wait(barrier, NZ - 1 + NXC - 1 + NT - 1)

    right = (t + 1) % NT
    left = (t + 3) % NT

    def w_piece(owner, piece, half=None):
        if piece < 2:
            buf = wgb if piece == 0 else wub
            if half is None:
                return buf.at[owner]
            return buf.at[owner, pl.ds(half * HALF, HALF)]
        if half is None:
            return wdb.at[piece - 2, owner]
        return wdb.at[piece - 2, owner, pl.ds(half * (UNITS // 2), UNITS // 2)]

    def w_source(piece):
        if piece == 0:
            return wg_hbm.at[0]
        if piece == 1:
            return wu_hbm.at[0]
        return wd_hbm.at[0, :, pl.ds((piece - 2) * CW, CW)]

    def w_own(way, piece):
        to = right if way == 0 else left
        return remote(
            w_source(piece),
            w_piece(t, piece),
            w_ss.at[way * (2 + NCH) + piece],
            w_rs.at[way * (2 + NCH) + piece],
            ep,
            to,
        )

    def w_forward(way, piece):
        owner = left if way == 0 else right
        to = right if way == 0 else left
        return remote(
            w_piece(owner, piece, way),
            w_piece(owner, piece, way),
            f_ss.at[way * (2 + NCH) + piece],
            f_rs.at[way * (2 + NCH) + piece],
            ep,
            to,
        )

    def send_piece(piece):
        for way in range(2):
            w_own(way, piece).start()

    def forward_piece(piece):
        for way in range(2):
            w_own(way, piece).wait_recv()
            w_forward(way, piece).start()

    def q_copy(j):
        return remote(q_hbm, qbuf.at[xc], q_ss.at[j], q_rs.at[j], xc_peer(j), t)

    def kv_copy(way, step, which):
        shift = 1 - step if way == 0 else step - 1
        slot = (z + NZ + shift) % NZ
        buf = vbuf if which else kbuf
        src = (v_hbm if which else k_hbm) if step == 1 else buf.at[slot]
        i = (way * 5 + step) * 2 + which
        return remote(
            src, buf.at[slot], kv_ss.at[i], kv_rs.at[i], z_peer(1 if way == 0 else NZ - 1), t
        )

    def kv_parts(step):
        if step < 4:
            return [(0, 0), (0, 1), (1, 0), (1, 1)]
        return [(0, 0), (1, 1)]
    send_piece(0)
    send_piece(1)
    for way, which in kv_parts(1):
        kv_copy(way, 1, which).start()
    for j in range(1, NXC):
        q_copy(j).start()

    def d1_copy(k):
        return remote(
            dsend.at[pl.ds(((z + k) % NZ) * NXC, NXC)],
            dmid.at[pl.ds(z * NXC, NXC)],
            d1_ss.at[k],
            d1_rs.at[k],
            z_peer(k),
            t,
        )

    def d2_copy(k, j):
        zs = (z + NZ - k) % NZ
        return remote(
            dmid.at[zs * NXC + (xc + j) % NXC],
            dout.at[zs * NXC + xc],
            d2_ss.at[0],
            d2_rs.at[j],
            xc_peer(j),
            t,
        )

    def o1_copy(h, k):
        return remote(
            osend.at[h, pl.ds(((z + k) % NZ) * NXC, NXC)],
            omid.at[h, pl.ds(z * NXC, NXC)],
            o1_ss.at[h * NZ + k],
            o1_rs.at[h * NZ + k],
            z_peer(k),
            t,
        )

    def o2_copy(h, k, j):
        zs = (z + NZ - k) % NZ
        return remote(
            omid.at[h, zs * NXC + (xc + j) % NXC],
            oret.at[h, zs * NXC + xc],
            o2_ss.at[h],
            o2_rs.at[h * NXC + j],
            xc_peer(j),
            t,
        )

    def d2_whole(j, count):
        return remote(
            dmid.at[pl.ds(0, count)],
            dout.at[pl.ds(0, count)],
            d2_ss.at[0],
            d2_rs.at[j],
            xc_peer(j),
            t,
        )

    def o2_whole(h, j, count):
        return remote(
            omid.at[h, pl.ds(0, count)],
            oret.at[h, pl.ds(0, count)],
            o2_ss.at[h],
            o2_rs.at[h * NXC + j],
            xc_peer(j),
            t,
        )

    def d2_stage(k):
        if k:
            d1_copy(k).wait_recv()

        @pl.loop(1, NXC)
        def _(j):
            d2_copy(k, j).start()

        zs = (z + NZ - k) % NZ
        dout[zs * NXC + xc] = dmid[zs * NXC + xc]

    dmid[pl.ds(z * NXC, NXC)] = dsend[pl.ds(z * NXC, NXC)]

    for step in range(1, 5):
        for way, which in kv_parts(step):
            kv_copy(way, step, which).wait_recv()
        if step < 4:
            for way, which in kv_parts(step + 1):
                kv_copy(way, step + 1, which).start()
        if step == 3:
            for k in Z_ORDER:
                d1_copy(k).start()

    for load in loads[1:4]:
        load.wait()
    for j in range(1, NXC):
        q_copy(j).wait_recv()

    lane = lax.broadcasted_iota(jnp.int32, (ROWS, 128), 1)

    def p_copy(j):
        return remote(
            psend.at[(xc + j) % NXC], precv.at[xc], p_ss.at[j], p_rs.at[j], xc_peer(j), t
        )

    def attend(j, dst):
        source = (xc + j) % NXC
        stats = jnp.zeros((ROWS, 128), F32)
        for h in range(2):
            cols = pl.ds(h * 128, 128)
            query = qbuf[source, :, cols].astype(F32) * 0.125
            keys = kbuf[:, :, cols].reshape(NZ * ROWS, 128)
            values = vbuf[:, :, cols].reshape(NZ * ROWS, 128)
            for m in range(2):
                own = (lane >= 64) if m else (lane < 64)
                masked = jnp.where(own, query, 0.0).astype(BF16)
                scores = lax.dot_general(
                    masked, keys, (((1,), (1,)), ((), ())), preferred_element_type=F32
                )
                top = jnp.max(scores, axis=1, keepdims=True)
                weights = jnp.exp(scores - top)
                total = jnp.sum(weights, axis=1, keepdims=True)
                summed = dot(weights.astype(BF16), values)
                i = h * 2 + m
                dst[:, pl.ds(i * 128, 128)] = (summed / total).astype(BF16)
                lse = top + jnp.log(total)
                high = lse.astype(BF16).astype(F32)
                mid = (lse - high).astype(BF16).astype(F32)
                low = lse - high - mid
                stats = jnp.where(lane == i, high, stats)
                stats = jnp.where(lane == 4 + i, mid, stats)
                stats = jnp.where(lane == 8 + i, low, stats)
        dst[:, pl.ds(512, 128)] = stats.astype(BF16)

    def attend_range(first, last):
        @pl.loop(first, last)
        def _(j):
            attend(j, psend.at[(xc + j) % NXC])
            p_copy(j).start()
    attend_range(1, 3)
    d2_stage(0)
    forward_piece(0)
    attend_range(3, 6)
    d2_stage(1)
    d2_stage(7)
    send_piece(2)
    send_piece(3)
    attend_range(6, NXC)
    attend(0, precv.at[xc])
    forward_piece(1)
    d2_stage(2)
    d2_stage(6)
    for j in range(1, NXC):
        p_copy(j).wait_recv()
    d2_stage(3)
    d2_stage(5)
    lses = []
    for d in range(NXC):
        stats = precv[d, :, pl.ds(512, 128)].astype(F32)
        lses.append(stats + pltpu.roll(stats, 124, 1) + pltpu.roll(stats, 120, 1))
    highest = lses[0]
    for d in range(1, NXC):
        highest = jnp.maximum(highest, lses[d])
    shares = [jnp.exp(lses[d] - highest) for d in range(NXC)]
    whole = shares[0]
    for d in range(1, NXC):
        whole = whole + shares[d]
    for d in range(NXC):
        shares[d] = shares[d] / whole
    for h in range(2):
        mixed = []
        for m in range(2):
            i = h * 2 + m
            acc = jnp.zeros((ROWS, 128), F32)
            for d in range(NXC):
                acc = acc + shares[d][:, i : i + 1] * precv[d, :, pl.ds(i * 128, 128)].astype(F32)
            mixed.append(acc)
        per_head = mixed[0] - lam_ref[h] * mixed[1]
        squared = jnp.mean(per_head * per_head, axis=1, keepdims=True)
        normed = per_head * lax.rsqrt(squared + EPS) * hg_ref[...] * HEAD_SCALE
        for y in range(NT):
            att[y, :, pl.ds(h * 128, 128)] = normed[y * 48 : (y + 1) * 48].astype(BF16)

    def a_copy(y):
        return remote(
            att.at[(t + y) % NT], attall.at[t], a_ss.at[y], a_rs.at[y], ep, (t + y) % NT
        )

    for y in range(1, NT):
        a_copy(y).start()
    attall[t] = att[t]
    d2_stage(4)
    forward_piece(2)
    forward_piece(3)
    send_piece(4)
    send_piece(5)
    for j in range(1, NXC):
        d2_whole(j, NZ).wait_recv()

    for load in loads[4:6]:
        load.wait()

    def hidden_block(r, off):
        b = (t + off) % NT
        arrived = xall[pl.ds(pl.multiple_of(r * 256, 256), 256), :]
        gate_part = dot(arrived, wgb[b])
        up_part = dot(arrived, wub[b])
        hidden = gate_part / (1.0 + jnp.exp(-gate_part)) * up_part
        hid[
            pl.ds(pl.multiple_of(r * 256, 256), 256), pl.ds(pl.multiple_of(b * UNITS, UNITS), UNITS)
        ] = hidden.astype(BF16)
    @pl.loop(0, 2)
    def _(r):
        xall[pl.ds(pl.multiple_of(r * 256, 256), 256), :] = dout[pl.ds(r * 32, 32)].reshape(256, D)
        for off in (0, 1, 3):
            hidden_block(r, off)
    for piece in range(2):
        for way in range(2):
            w_forward(way, piece).wait_recv()
    @pl.loop(0, 2)
    def _(r):
        hidden_block(r, 2)

    def down(h):
        loads[7 + h].wait()
        for way in range(2):
            w_forward(way, 2 + h).wait_recv()

        @pl.loop(0, 2)
        def _(r):
            part = hid[pl.ds(pl.multiple_of(r * 256, 256), 256), :]
            result = dot(part, wdb[h].reshape(NT * UNITS, CW))
            osend[h, pl.ds(r * 32, 32)] = result.reshape(32, CAP, CW).astype(BF16)

        for k in Z_ORDER:
            o1_copy(h, k).start()
        omid[h, pl.ds(z * NXC, NXC)] = osend[h, pl.ds(z * NXC, NXC)]

    def o2_stage(h, k):
        if k:
            o1_copy(h, k).wait_recv()

        @pl.loop(1, NXC)
        def _(j):
            o2_copy(h, k, j).start()

        zs = (z + NZ - k) % NZ
        oret[h, zs * NXC + xc] = omid[h, zs * NXC + xc]

    def o2_stages(h):
        for k in (0,) + Z_ORDER:
            o2_stage(h, k)

    def combine(h):
        for j in range(1, NXC):
            o2_whole(h, j, NZ).wait_recv()

        result = dot(gmat[...], oret[h].reshape(SLOTS, CW))
        moe_ref[:, pl.ds(h * CW, CW)] = (result[:TOK] + result[TOK:]).astype(BF16)

    def project():
        loads[6].wait()
        for y in range(1, NT):
            a_copy(y).wait_recv()
        for c in range(4):
            cols = pl.ds(c * 512, 512)
            acc = dot(attall[0], wob[pl.ds(0, 256), cols])
            for y in range(1, NT):
                acc = acc + dot(attall[y], wob[pl.ds(y * 256, 256), cols])
            mix_ref[:, cols] = acc.astype(BF16)

    for h in range(NCH):
        down(h)
        if h + 2 < NCH:
            forward_piece(2 + h + 2)
        if h + 4 < NCH:
            send_piece(2 + h + 4)
        if h >= 2:
            o2_stages(h - 2)
        if h >= 4:
            combine(h - 4)
    project()
    o2_stages(NCH - 2)
    combine(NCH - 4)
    combine(NCH - 3)
    o2_stages(NCH - 1)
    combine(NCH - 2)
    combine(NCH - 1)
    for j in range(1, NXC):
        q_copy(j).wait_send()
        p_copy(j).wait_send()
    for step in range(1, 5):
        for way, which in kv_parts(step):
            kv_copy(way, step, which).wait_send()
    for k in range(1, NZ):
        d1_copy(k).wait_send()
        for h in range(NCH):
            o1_copy(h, k).wait_send()
    for y in range(1, NT):
        a_copy(y).wait_send()
    for way in range(2):
        for piece in range(2 + NCH):
            w_own(way, piece).wait_send()
            w_forward(way, piece).wait_send()

    d2_whole(1, 56).wait_send()
    for h in range(NCH):
        o2_whole(h, 1, 56).wait_send()


def local(
    query_rows,
    key_rows,
    value_rows,
    lambdas,
    head_gain,
    w_out,
    moe_rows,
    ffn_gain,
    routes,
    group_logits,
    pick_logits,
    w_gate,
    w_up,
    w_down,
):
    any_ = pl.BlockSpec(memory_space=pl.ANY)
    vmem = pl.BlockSpec(memory_space=pltpu.VMEM)
    smem = pl.BlockSpec(memory_space=pltpu.SMEM)
    dma = pltpu.SemaphoreType.DMA
    return pl.pallas_call(
        kernel,
        out_shape=(
            jax.ShapeDtypeStruct((ROWS // NT, D), BF16),
            jax.ShapeDtypeStruct((TOK, D), BF16),
        ),
        in_specs=[any_, any_, any_, smem, vmem, any_, any_, vmem, vmem, vmem, vmem, any_, any_, any_],
        out_specs=(vmem, vmem),
        scratch_shapes=[
            pltpu.VMEM((NXC, ROWS, 256), BF16),
            pltpu.VMEM((NZ, ROWS, 256), BF16),
            pltpu.VMEM((NZ, ROWS, 256), BF16),
            pltpu.VMEM((NXC, ROWS, 640), BF16),
            pltpu.VMEM((NXC, ROWS, 640), BF16),
            pltpu.VMEM((NT, 48, 256), BF16),
            pltpu.VMEM((NT, 48, 256), BF16),
            pltpu.VMEM((1024, D), BF16),
            pltpu.VMEM((TOK, D), BF16),
            pltpu.VMEM((2 * TOK, SLOTS), BF16),
            pltpu.VMEM((EXPERTS, CAP, D), BF16),
            pltpu.VMEM((EXPERTS, CAP, D), BF16),
            pltpu.VMEM((EXPERTS, CAP, D), BF16),
            pltpu.VMEM((SLOTS, D), BF16),
            pltpu.VMEM((NT, D, UNITS), BF16),
            pltpu.VMEM((NT, D, UNITS), BF16),
            pltpu.VMEM((NCH, NT, UNITS, CW), BF16),
            pltpu.VMEM((SLOTS, 1024), BF16),
            pltpu.VMEM((NCH, EXPERTS, CAP, CW), BF16),
            pltpu.VMEM((NCH, EXPERTS, CAP, CW), BF16),
            pltpu.VMEM((NCH, EXPERTS, CAP, CW), BF16),
            dma((15,)),
            dma((NXC,)),
            dma((NXC,)),
            dma((20,)),
            dma((20,)),
            dma((NXC,)),
            dma((NXC,)),
            dma((NT,)),
            dma((NT,)),
            dma((2 * (2 + NCH),)),
            dma((2 * (2 + NCH),)),
            dma((2 * (2 + NCH),)),
            dma((2 * (2 + NCH),)),
            dma((NZ,)),
            dma((NZ,)),
            dma((1,)),
            dma((NXC,)),
            dma((NCH * NZ,)),
            dma((NCH * NZ,)),
            dma((NCH,)),
            dma((NCH * NXC,)),
        ],
        compiler_params=pltpu.CompilerParams(
            collective_id=0, has_side_effects=True, vmem_limit_bytes=66_000_000
        ),
    )(
        query_rows,
        key_rows,
        value_rows,
        lambdas,
        head_gain[None],
        w_out,
        moe_rows,
        ffn_gain[None],
        routes.T,
        group_logits.T,
        pick_logits.T,
        w_gate,
        w_up,
        w_down,
    )


def solution(mesh):
    return jax.shard_map(
        local,
        mesh=mesh,
        in_specs=(
            P("ep", "tp"),
            P("ep", "tp"),
            P("ep", "tp"),
            P("tp"),
            P(),
            P(),
            P("ep", None),
            P(),
            P("ep", None),
            P("ep", None),
            P("ep", None),
            P("ep", None, "tp"),
            P("ep", None, "tp"),
            P("ep", "tp", None),
        ),
        out_specs=(P(("ep", "tp"), None), P(("ep", "tp"), None)),
        check_vma=False,
    )
```

time: 178 us -> 150 us (0.84)
  Pallas kernels: 169 us -> 146 us
  local copies, waits for them, and re-layouts: 8.12 us -> 3.5 us
    pallas_call x1, Pallas kernels: 169 us -> 146 us  [local(): pl.pallas_call(kernel, out_shape=(jax.ShapeDtypeStruct((ROWS // NT, D), B...]
    unnamed x5 -> x2, local copies, waits for them, and re-layouts: 8.12 us -> 3.5 us
where the time goes in v2:
time: 150 us
  Pallas kernels  146 us (97%)
  local copies, waits for them, and re-layouts  3.5 us (2%)
    pallas_call x1, Pallas kernels, local(): pl.pallas_call(kernel, out_shape=(jax.ShapeDtypeStruct((ROWS // NT, D), B...  146 us
    unnamed x2, local copies, waits for them, and re-layouts  3.5 us

profile of v2, /device:TPU:1, one launch (start us, length us, event | category | flops | bytes accessed | tf_op | source)
XLA Modules:
  0.0 149.8 jit_solution(9493515121072687092)
XLA Ops:
  0.6 145.7 %shard_map.149 = (bf16[48,2048]{1,0:T(8,128)(2,1)}, bf16[128,2048]{1,0:T(8,128)(2,1)}) custom-call(bf16[192,256]{1,0:T(8,128)(2,1)} %q_hbm.1, bf16[192,256]{1,0:T(8,128)(2,1)} %k_hbm.1, bf16[192,256]{1,0:T(8,128)(2,1)} %v_hbm.1, f32[2]{0:T(128)} %lam_ref.1, f32[1,128]{1,0:T(1,128)} %bitcast.9, bf16[1024,2048]{1,0:T(8,128)(2,1)} %wo_hbm.1, ...), custom_call_target="tpu_custom_call" | custom-call | tf_op jit(solution)/shard_map/pallas_call | solution.py:577
  146.3 1.6 %copy.18 = bf16[48,2048]{1,0:T(8,128)(2,1)} copy(bf16[48,2048]{1,0:T(8,128)(2,1)} %get-tuple-element.4) | data formatting | bytes 393216
  147.9 1.9 %copy.19 = bf16[128,2048]{1,0:T(8,128)(2,1)} copy(bf16[128,2048]{1,0:T(8,128)(2,1)} %get-tuple-element.5) | data formatting | bytes 1048576

commit v3 on v2

--- a/solution.py
+++ b/solution.py
@@ -19,6 +19,9 @@
 UNITS = 256
 SLOTS = EXPERTS * CAP
 Z_ORDER = (1, 7, 2, 6, 3, 5, 4)
+ROW_ORDER = (0,) + Z_ORDER
+NEAR = ROW_ORDER[:5]
+ZROWS = NXC * CAP
 F32 = jnp.float32
 BF16 = jnp.bfloat16
 MESH = pl.DeviceIdType.MESH
@@ -92,6 +95,7 @@
     t = lax.axis_index("tp")
     z = ep // NXC
     xc = ep % NXC
+    core = ep % 2
 
     def z_peer(k):
         return ((z + k) % NZ) * NXC + xc
@@ -241,14 +245,32 @@
             src, buf.at[slot], kv_ss.at[i], kv_rs.at[i], z_peer(1 if way == 0 else NZ - 1), t
         )
 
+    def d1_part(k, part):
+        return remote(
+            dsend.at[pl.ds(((z + k) % NZ) * NXC + part * 2, 2)],
+            dmid.at[pl.ds(z * NXC + part * 2, 2)],
+            d1_ss.at[k],
+            d1_rs.at[k],
+            z_peer(k),
+            t,
+        )
+
+    def d1_parts(part):
+        d1_part(1, part).start()
+        d1_part(7, part).start()
+
     def kv_parts(step):
         if step < 4:
             return [(0, 0), (0, 1), (1, 0), (1, 1)]
         return [(0, 0), (1, 1)]
-    send_piece(0)
-    send_piece(1)
+    @pl.when(core == 0)
+    def _():
+        send_piece(0)
+        send_piece(1)
+
     for way, which in kv_parts(1):
         kv_copy(way, 1, which).start()
+    d1_parts(0)
     for j in range(1, NXC):
         q_copy(j).start()
 
@@ -268,7 +290,7 @@
             dmid.at[zs * NXC + (xc + j) % NXC],
             dout.at[zs * NXC + xc],
             d2_ss.at[0],
-            d2_rs.at[j],
+            d2_rs.at[j if k in NEAR else NXC + j],
             xc_peer(j),
             t,
         )
@@ -294,12 +316,12 @@
             t,
         )
 
-    def d2_whole(j, count):
+    def d2_whole(j, count, far=0):
         return remote(
             dmid.at[pl.ds(0, count)],
             dout.at[pl.ds(0, count)],
             d2_ss.at[0],
-            d2_rs.at[j],
+            d2_rs.at[far * NXC + j],
             xc_peer(j),
             t,
         )
@@ -333,9 +355,22 @@
         if step < 4:
             for way, which in kv_parts(step + 1):
                 kv_copy(way, step + 1, which).start()
+        if step < 4:
+            d1_parts(step)
+        if step == 2:
+
+            @pl.when(core == 0)
+            def _():
+                forward_piece(0)
+
         if step == 3:
-            for k in Z_ORDER:
+            for k in Z_ORDER[2:]:
                 d1_copy(k).start()
+    @pl.when(core == 0)
+    def _():
+        forward_piece(1)
+        for h in range(NCH):
+            send_piece(2 + h)
 
     for load in loads[1:4]:
         load.wait()
@@ -378,105 +413,146 @@
                 stats = jnp.where(lane == 8 + i, low, stats)
         dst[:, pl.ds(512, 128)] = stats.astype(BF16)
 
-    def attend_range(first, last):
+    def attend_range(first, last, sent):
         @pl.loop(first, last)
         def _(j):
             attend(j, psend.at[(xc + j) % NXC])
-            p_copy(j).start()
-    attend_range(1, 3)
-    d2_stage(0)
-    forward_piece(0)
-    attend_range(3, 6)
-    d2_stage(1)
-    d2_stage(7)
-    send_piece(2)
-    send_piece(3)
-    attend_range(6, NXC)
-    attend(0, precv.at[xc])
-    forward_piece(1)
+            if sent:
+                p_copy(j).start()
+    attend_range(1, 3, True)
+    for k in (0, 1, 7):
+        d2_stage(k)
+    attend_range(3, 6, True)
     d2_stage(2)
     d2_stage(6)
-    for j in range(1, NXC):
-        p_copy(j).wait_recv()
+    attend_range(6, NXC, False)
+    attend(0, precv.at[xc])
+
+    @pl.when(core == 1)
+    def _():
+        send_piece(0)
+        send_piece(1)
+        send_piece(2)
+    @pl.when(core == 0)
+    def _():
+        for h in range(NCH // 2):
+            forward_piece(2 + h)
     d2_stage(3)
     d2_stage(5)
-    lses = []
-    for d in range(NXC):
-        stats = precv[d, :, pl.ds(512, 128)].astype(F32)
-        lses.append(stats + pltpu.roll(stats, 124, 1) + pltpu.roll(stats, 120, 1))
-    highest = lses[0]
-    for d in range(1, NXC):
-        highest = jnp.maximum(highest, lses[d])
-    shares = [jnp.exp(lses[d] - highest) for d in range(NXC)]
-    whole = shares[0]
-    for d in range(1, NXC):
-        whole = whole + shares[d]
-    for d in range(NXC):
-        shares[d] = shares[d] / whole
-    for h in range(2):
-        mixed = []
-        for m in range(2):
-            i = h * 2 + m
-            acc = jnp.zeros((ROWS, 128), F32)
-            for d in range(NXC):
-                acc = acc + shares[d][:, i : i + 1] * precv[d, :, pl.ds(i * 128, 128)].astype(F32)
-            mixed.append(acc)
-        per_head = mixed[0] - lam_ref[h] * mixed[1]
-        squared = jnp.mean(per_head * per_head, axis=1, keepdims=True)
-        normed = per_head * lax.rsqrt(squared + EPS) * hg_ref[...] * HEAD_SCALE
-        for y in range(NT):
-            att[y, :, pl.ds(h * 128, 128)] = normed[y * 48 : (y + 1) * 48].astype(BF16)
+    @pl.when(core == 0)
+    def _():
+        for h in range(NCH // 2, NCH):
+            forward_piece(2 + h)
+    d2_stage(4)
+
+    for j in range(6, NXC):
+        p_copy(j).start()
 
     def a_copy(y):
         return remote(
             att.at[(t + y) % NT], attall.at[t], a_ss.at[y], a_rs.at[y], ep, (t + y) % NT
         )
 
-    for y in range(1, NT):
-        a_copy(y).start()
-    attall[t] = att[t]
-    d2_stage(4)
-    forward_piece(2)
-    forward_piece(3)
-    send_piece(4)
-    send_piece(5)
-    for j in range(1, NXC):
-        d2_whole(j, NZ).wait_recv()
+    def merge():
+        for j in range(1, NXC):
+            p_copy(j).wait_recv()
+        lses = []
+        for d in range(NXC):
+            stats = precv[d, :, pl.ds(512, 128)].astype(F32)
+            lses.append(stats + pltpu.roll(stats, 124, 1) + pltpu.roll(stats, 120, 1))
+        highest = lses[0]
+        for d in range(1, NXC):
+            highest = jnp.maximum(highest, lses[d])
+        shares = [jnp.exp(lses[d] - highest) for d in range(NXC)]
+        whole = shares[0]
+        for d in range(1, NXC):
+            whole = whole + shares[d]
+        for d in range(NXC):
+            shares[d] = shares[d] / whole
+        for h in range(2):
+            mixed = []
+            for m in range(2):
+                i = h * 2 + m
+                acc = jnp.zeros((ROWS, 128), F32)
+                for d in range(NXC):
+                    acc = acc + shares[d][:, i : i + 1] * precv[d, :, pl.ds(i * 128, 128)].astype(F32)
+                mixed.append(acc)
+            per_head = mixed[0] - lam_ref[h] * mixed[1]
+            squared = jnp.mean(per_head * per_head, axis=1, keepdims=True)
+            normed = per_head * lax.rsqrt(squared + EPS) * hg_ref[...] * HEAD_SCALE
+            for y in range(NT):
+                att[y, :, pl.ds(h * 128, 128)] = normed[y * 48 : (y + 1) * 48].astype(BF16)
+
+        for y in range(1, NT):
+            a_copy(y).start()
+        attall[t] = att[t]
+    @pl.when(core == 1)
+    def _():
+        forward_piece(0)
+        forward_piece(1)
+        forward_piece(2)
+        send_piece(3)
+        send_piece(4)
 
     for load in loads[4:6]:
         load.wait()
 
-    def hidden_block(r, off):
+    def take_rows(far):
+        first, last = (5, NZ) if far else (0, 5)
+        for j in range(1, NXC):
+            d2_whole(j, last - first, far).wait_recv()
+        for i in range(first, last):
+            zs = (z + NZ - ROW_ORDER[i]) % NZ
+            xall[pl.ds(i * ZROWS, ZROWS), :] = dout[pl.ds(zs * NXC, NXC)].reshape(ZROWS, D)
+
+    def hidden_block(far, off):
+        rows = pl.ds(5 * ZROWS, 3 * ZROWS) if far else pl.ds(0, 5 * ZROWS)
         b = (t + off) % NT
-        arrived = xall[pl.ds(pl.multiple_of(r * 256, 256), 256), :]
+        arrived = xall[rows, :]
         gate_part = dot(arrived, wgb[b])
         up_part = dot(arrived, wub[b])
         hidden = gate_part / (1.0 + jnp.exp(-gate_part)) * up_part
-        hid[
-            pl.ds(pl.multiple_of(r * 256, 256), 256), pl.ds(pl.multiple_of(b * UNITS, UNITS), UNITS)
-        ] = hidden.astype(BF16)
-    @pl.loop(0, 2)
-    def _(r):
-        xall[pl.ds(pl.multiple_of(r * 256, 256), 256), :] = dout[pl.ds(r * 32, 32)].reshape(256, D)
-        for off in (0, 1, 3):
-            hidden_block(r, off)
-    for piece in range(2):
-        for way in range(2):
-            w_forward(way, piece).wait_recv()
-    @pl.loop(0, 2)
-    def _(r):
-        hidden_block(r, 2)
+        hid[rows, pl.ds(pl.multiple_of(b * UNITS, UNITS), UNITS)] = hidden.astype(BF16)
+
+    def opposite_weights():
+        for piece in range(2):
+            for way in range(2):
+                w_forward(way, piece).wait_recv()
+    take_rows(0)
+    for off in (0, 1, 3):
+        hidden_block(0, off)
+
+    @pl.when(core == 0)
+    def _():
+        opposite_weights()
+        hidden_block(0, 2)
+    take_rows(1)
+    for off in (0, 1, 3):
+        hidden_block(1, off)
+    @pl.when(core == 1)
+    def _():
+        merge()
+    @pl.when(core == 1)
+    def _():
+        opposite_weights()
+        hidden_block(0, 2)
+    hidden_block(1, 2)
+    @pl.when(core == 1)
+    def _():
+        forward_piece(3)
+        send_piece(5)
 
     def down(h):
         loads[7 + h].wait()
         for way in range(2):
             w_forward(way, 2 + h).wait_recv()
 
-        @pl.loop(0, 2)
-        def _(r):
-            part = hid[pl.ds(pl.multiple_of(r * 256, 256), 256), :]
-            result = dot(part, wdb[h].reshape(NT * UNITS, CW))
-            osend[h, pl.ds(r * 32, 32)] = result.reshape(32, CAP, CW).astype(BF16)
+        for r in range(2):
+            result = dot(hid[pl.ds(r * 256, 256), :], wdb[h].reshape(NT * UNITS, CW))
+            for i in range(4):
+                zs = (z + NZ - ROW_ORDER[r * 4 + i]) % NZ
+                block = result[i * ZROWS : (i + 1) * ZROWS].reshape(NXC, CAP, CW)
+                osend[h, pl.ds(zs * NXC, NXC)] = block.astype(BF16)
 
         for k in Z_ORDER:
             o1_copy(h, k).start()
@@ -514,22 +590,33 @@
             for y in range(1, NT):
                 acc = acc + dot(attall[y], wob[pl.ds(y * 256, 256), cols])
             mix_ref[:, cols] = acc.astype(BF16)
-
-    for h in range(NCH):
-        down(h)
-        if h + 2 < NCH:
-            forward_piece(2 + h + 2)
-        if h + 4 < NCH:
-            send_piece(2 + h + 4)
-        if h >= 2:
-            o2_stages(h - 2)
-        if h >= 4:
-            combine(h - 4)
-    project()
-    o2_stages(NCH - 2)
-    combine(NCH - 4)
-    combine(NCH - 3)
-    o2_stages(NCH - 1)
+    @pl.when(core == 0)
+    def _():
+        for h in range(NCH):
+            down(h)
+        merge()
+        for h in range(NCH):
+            o2_stages(h)
+        project()
+    @pl.when(core == 1)
+    def _():
+        for h in range(NCH):
+            down(h)
+            if h + 2 < NCH:
+                forward_piece(2 + h + 2)
+            if h + 4 < NCH:
+                send_piece(2 + h + 4)
+            if h >= 3:
+                o2_stages(h - 3)
+            if h == 4:
+                project()
+        o2_stages(NCH - 3)
+        o2_stages(NCH - 2)
+    for h in range(NCH - 2):
+        combine(h)
+    @pl.when(core == 1)
+    def _():
+        o2_stages(NCH - 1)
     combine(NCH - 2)
     combine(NCH - 1)
     for j in range(1, NXC):
@@ -620,7 +707,7 @@
             dma((NZ,)),
             dma((NZ,)),
             dma((1,)),
-            dma((NXC,)),
+            dma((2 * NXC,)),
             dma((NCH * NZ,)),
             dma((NCH * NZ,)),
             dma((NCH,)),

time: 150 us -> 143 us (0.953)
  Pallas kernels: 146 us -> 139 us
    pallas_call x1, Pallas kernels: 146 us -> 139 us  [local(): pl.pallas_call(kernel, out_shape=(jax.ShapeDtypeStruct((ROWS // NT, D), B...]
where the time goes in v3:
time: 143 us
  Pallas kernels  139 us (97%)
  local copies, waits for them, and re-layouts  3.5 us (2%)
    pallas_call x1, Pallas kernels, local(): pl.pallas_call(kernel, out_shape=(jax.ShapeDtypeStruct((ROWS // NT, D), B...  139 us
    unnamed x2, local copies, waits for them, and re-layouts  3.5 us

profile of v3, /device:TPU:1, one launch (start us, length us, event | category | flops | bytes accessed | tf_op | source)
XLA Modules:
  0.0 142.9 jit_solution(1961025564123464385)
XLA Ops:
  0.6 138.8 %shard_map.149 = (bf16[48,2048]{1,0:T(8,128)(2,1)}, bf16[128,2048]{1,0:T(8,128)(2,1)}) custom-call(bf16[192,256]{1,0:T(8,128)(2,1)} %q_hbm.1, bf16[192,256]{1,0:T(8,128)(2,1)} %k_hbm.1, bf16[192,256]{1,0:T(8,128)(2,1)} %v_hbm.1, f32[2]{0:T(128)} %lam_ref.1, f32[1,128]{1,0:T(1,128)} %bitcast.9, bf16[1024,2048]{1,0:T(8,128)(2,1)} %wo_hbm.1, ...), custom_call_target="tpu_custom_call" | custom-call | tf_op jit(solution)/shard_map/pallas_call | solution.py:664
  139.4 1.6 %copy.18 = bf16[48,2048]{1,0:T(8,128)(2,1)} copy(bf16[48,2048]{1,0:T(8,128)(2,1)} %get-tuple-element.4) | data formatting | bytes 393216
  141.0 1.9 %copy.19 = bf16[128,2048]{1,0:T(8,128)(2,1)} copy(bf16[128,2048]{1,0:T(8,128)(2,1)} %get-tuple-element.5) | data formatting | bytes 1048576

commit v4 on v3

--- a/solution.py
+++ b/solution.py
@@ -518,6 +518,23 @@
         for piece in range(2):
             for way in range(2):
                 w_forward(way, piece).wait_recv()
+
+    def down(h, far):
+        if not far:
+            loads[7 + h].wait()
+            for way in range(2):
+                w_forward(way, 2 + h).wait_recv()
+        first, last = (5, NZ) if far else (0, 5)
+        rows = pl.ds(first * ZROWS, (last - first) * ZROWS)
+        result = dot(hid[rows, :], wdb[h].reshape(NT * UNITS, CW))
+        for i in range(first, last):
+            zs = (z + NZ - ROW_ORDER[i]) % NZ
+            block = result[(i - first) * ZROWS : (i - first + 1) * ZROWS].reshape(NXC, CAP, CW)
+            osend[h, pl.ds(zs * NXC, NXC)] = block.astype(BF16)
+        for k in ROW_ORDER[max(first, 1) : last]:
+            o1_copy(h, k).start()
+        if not far:
+            omid[h, pl.ds(z * NXC, NXC)] = osend[h, pl.ds(z * NXC, NXC)]
     take_rows(0)
     for off in (0, 1, 3):
         hidden_block(0, off)
@@ -526,6 +543,8 @@
     def _():
         opposite_weights()
         hidden_block(0, 2)
+        for h in range(NCH):
+            down(h, 0)
     take_rows(1)
     for off in (0, 1, 3):
         hidden_block(1, off)
@@ -541,22 +560,6 @@
     def _():
         forward_piece(3)
         send_piece(5)
-
-    def down(h):
-        loads[7 + h].wait()
-        for way in range(2):
-            w_forward(way, 2 + h).wait_recv()
-
-        for r in range(2):
-            result = dot(hid[pl.ds(r * 256, 256), :], wdb[h].reshape(NT * UNITS, CW))
-            for i in range(4):
-                zs = (z + NZ - ROW_ORDER[r * 4 + i]) % NZ
-                block = result[i * ZROWS : (i + 1) * ZROWS].reshape(NXC, CAP, CW)
-                osend[h, pl.ds(zs * NXC, NXC)] = block.astype(BF16)
-
-        for k in Z_ORDER:
-            o1_copy(h, k).start()
-        omid[h, pl.ds(z * NXC, NXC)] = osend[h, pl.ds(z * NXC, NXC)]
 
     def o2_stage(h, k):
         if k:
@@ -593,7 +596,7 @@
     @pl.when(core == 0)
     def _():
         for h in range(NCH):
-            down(h)
+            down(h, 1)
         merge()
         for h in range(NCH):
             o2_stages(h)
@@ -601,7 +604,8 @@
     @pl.when(core == 1)
     def _():
         for h in range(NCH):
-            down(h)
+            down(h, 0)
+            down(h, 1)
             if h + 2 < NCH:
                 forward_piece(2 + h + 2)
             if h + 4 < NCH:

time: 143 us -> 141 us (0.986)
  Pallas kernels: 139 us -> 137 us
    pallas_call x1, Pallas kernels: 139 us -> 137 us  [local(): pl.pallas_call(kernel, out_shape=(jax.ShapeDtypeStruct((ROWS // NT, D), B...]
where the time goes in v4:
time: 141 us
  Pallas kernels  137 us (97%)
  local copies, waits for them, and re-layouts  3.5 us (2%)
    pallas_call x1, Pallas kernels, local(): pl.pallas_call(kernel, out_shape=(jax.ShapeDtypeStruct((ROWS // NT, D), B...  137 us
    unnamed x2, local copies, waits for them, and re-layouts  3.5 us

profile of v4, /device:TPU:1, one launch (start us, length us, event | category | flops | bytes accessed | tf_op | source)
XLA Modules:
  0.0 141.2 jit_solution(13867818783418139514)
XLA Ops:
  0.6 137.0 %shard_map.149 = (bf16[48,2048]{1,0:T(8,128)(2,1)}, bf16[128,2048]{1,0:T(8,128)(2,1)}) custom-call(bf16[192,256]{1,0:T(8,128)(2,1)} %q_hbm.1, bf16[192,256]{1,0:T(8,128)(2,1)} %k_hbm.1, bf16[192,256]{1,0:T(8,128)(2,1)} %v_hbm.1, f32[2]{0:T(128)} %lam_ref.1, f32[1,128]{1,0:T(1,128)} %bitcast.9, bf16[1024,2048]{1,0:T(8,128)(2,1)} %wo_hbm.1, ...), custom_call_target="tpu_custom_call" | custom-call | tf_op jit(solution)/shard_map/pallas_call | solution.py:668
  137.7 1.6 %copy.18 = bf16[48,2048]{1,0:T(8,128)(2,1)} copy(bf16[48,2048]{1,0:T(8,128)(2,1)} %get-tuple-element.4) | data formatting | bytes 393216
  139.3 1.9 %copy.19 = bf16[128,2048]{1,0:T(8,128)(2,1)} copy(bf16[128,2048]{1,0:T(8,128)(2,1)} %get-tuple-element.5) | data formatting | bytes 1048576
